TPU v7x, 32 devices: a whole 2x2x4 slice. The times are simulated.
32 devices in a mesh: sp: 8 (over z, y), tp: 4 (over x, core).
Axes of the slice: x: 2, y: 2, z: 4, core: 2. Of those that a mesh axis runs over, the one named last changes fastest.
Arguments:
- tokens: bfloat16 [1024, 2048], P(('sp', 'tp')), may hold values from -6 to 6
- norm_gain: float32 [2048], replicated, may hold values from 0.1 to 1.9
- w_query: bfloat16 [2048, 1024], P(None, 'tp'), may hold values from -3 to 3
- w_key: bfloat16 [2048, 1024], P(None, 'tp'), may hold values from -0.15625 to 0.15625
- w_value: bfloat16 [2048, 1024], P(None, 'tp'), may hold values from -0.125 to 0.125
- w_state_in: bfloat16 [2048, 512], P(None, 'tp'), may hold values from -0.125 to 0.125
- decay_rate: float32 [32, 64], P('tp'), may hold values from 0 to 0.04, as said below
- rotation: float32 [32, 64], P('tp'), may hold values from -0.5 to 0.5
- extra_decay: float32 [1024, 32], P('sp', 'tp'), may hold values from -1 to 0, as said below
- in_map: float32 [2, 32, 64, 16], P(None, 'tp'), may hold values from -1 to 1
- out_map: float32 [2, 32, 16, 64], P(None, 'tp'), may hold values from -0.5 to 0.5
- skip_gain: float32 [32, 16], P('tp'), may hold values from -4 to 4
- init_state: float32 [1, 2, 32, 64], P(None, None, 'tp'), may hold values from -6 to 6
- mix_lambda: float32 [8], P('tp'), may hold values from 0.3 to 0.8
- sub_gain: float32 [128], replicated, may hold values from 0.1 to 1.9
- w_out_state: bfloat16 [512, 2048], P('tp', 'sp'), may hold values from -0.375 to 0.375
- w_out_attn: bfloat16 [1024, 2048], P('tp', 'sp'), may hold values from -0.1875 to 0.1875
Outputs:
- mixed_out: bfloat16 [1024, 2048], P(('sp', 'tp'))
Inputs may be any that keep to these rules, and one draw needn't show every extreme that they name: `decay_rate`: positive. `extra_decay`: never positive.
All inputs are finite; a program needn't handle non-finite values.
Results may differ from a plain program's by a relative error of at most 0.017.
The roundings to bfloat16 on the way count: a program that leaves them out, or rounds other values in their place, can miss the bound.
Values may be sent and summed in bfloat16 or wider, within the bound.
A program may use at most 128 MiB of HBM per device.

v0:
```python
import functools

import jax
import jax.numpy as jnp
from jax import lax
from jax.experimental import pallas as pl
from jax.experimental.pallas import tpu as pltpu
from jax.sharding import PartitionSpec as P

QK_DIM = 64
V_DIM = 128
SEGMENT = 64
EPSILON = 1e-06
ROTARY_BASE = 10000.0
LAMBDA_INIT = 0.2
MASK_FLOOR = -1e30
F32 = jnp.float32
BF16 = jnp.bfloat16
MESH = pl.DeviceIdType.MESH
HIGHEST = lax.Precision.HIGHEST
EARLY = 3


def dot(a, b, precision=None):
    return jnp.dot(a, b, preferred_element_type=F32, precision=precision)


def dot_t(a, b, precision=None):
    return lax.dot_general(
        a, b, (((1,), (1,)), ((), ())), preferred_element_type=F32, precision=precision
    )


def iota(shape, axis):
    return lax.broadcasted_iota(jnp.int32, shape, axis)


def kernel(
    cfg,
    tokens,
    gain,
    wq_hbm,
    wk_hbm,
    wv_hbm,
    wd_hbm,
    table,
    params,
    extra,
    in_map,
    out_map,
    skip,
    mix,
    sub_gain,
    ws_hbm,
    wa_hbm,
    out,
    xall,
    wq,
    wk,
    wv,
    wd,
    wos,
    woa,
    qz,
    kv,
    summary,
    tr,
    ti,
    ir,
    ii,
    peak,
    total,
    numer,
    part,
    landed,
    acts,
    local_sem,
    x_send,
    x_recv,
    w_send,
    w_recv,
    k_send,
    k_recv,
    s_send,
    s_recv,
    r_send,
    r_recv,
):
    seqs, chain, tps, slots = cfg
    sp = lax.axis_index("sp")
    tp = lax.axis_index("tp")
    li = sp // seqs
    seq = sp % seqs
    own, width = tokens.shape
    rows = own * tps
    heads = wv.shape[1] // V_DIM
    qw = wq.shape[1]
    cols = wos.shape[2]
    flat = tr.shape[1]
    groups = extra.shape[1]
    states = flat // groups
    chans = wd.shape[1]
    per = chans // groups

    pulls = [
        pltpu.make_async_copy(src, dst, local_sem.at[i])
        for i, (src, dst) in enumerate(
            (
                (ws_hbm, wos.at[0]),
                (wa_hbm, woa.at[0]),
                (wd_hbm, wd),
                (wk_hbm, wk),
                (wv_hbm, wv),
                (wq_hbm, wq),
            )
        )
    ]
    for pull in pulls:
        pull.start()

    barrier = pltpu.get_barrier_semaphore()

    def greet_tp(d, _):
        pl.semaphore_signal(
            barrier, inc=1, device_id={"tp": lax.rem(tp + d, tps)}, device_id_type=MESH
        )
        return 0

    def greet_sp(d, _):
        pl.semaphore_signal(
            barrier,
            inc=1,
            device_id={"sp": lax.rem(li + d, chain) * seqs + seq},
            device_id_type=MESH,
        )
        return 0

    lax.fori_loop(1, tps, greet_tp, 0)
    lax.fori_loop(1, chain, greet_sp, 0)

    wide = tokens[...].astype(F32)
    scale = lax.rsqrt(jnp.mean(wide * wide, axis=-1, keepdims=True) + EPSILON)
    xall[tp] = (wide * scale * gain[...]).astype(BF16)

    pl.semaphore_wait(barrier, tps - 1 + chain - 1)

    def x_copy(d):
        return pltpu.make_async_remote_copy(
            src_ref=xall.at[tp],
            dst_ref=xall.at[tp],
            send_sem=x_send.at[d],
            recv_sem=x_recv.at[d],
            device_id={"tp": lax.rem(tp + d, tps)},
            device_id_type=MESH,
        )

    def x_arrival(d):
        source = lax.rem(tp + tps - d, tps)
        return pltpu.make_async_remote_copy(
            src_ref=xall.at[tp],
            dst_ref=xall.at[source],
            send_sem=x_send.at[d],
            recv_sem=x_recv.at[d],
            device_id={"tp": source},
            device_id_type=MESH,
        )

    def w_copies(d):
        peer = {"sp": lax.rem(li + d, chain) * seqs + seq}
        return [
            pltpu.make_async_remote_copy(
                src_ref=ref.at[0],
                dst_ref=ref.at[d],
                send_sem=w_send.at[which, d],
                recv_sem=w_recv.at[which, d],
                device_id=peer,
                device_id_type=MESH,
            )
            for which, ref in enumerate((wos, woa))
        ]

    def chain_copy(ref, send, recv, d):
        return pltpu.make_async_remote_copy(
            src_ref=ref.at[0],
            dst_ref=ref.at[d],
            send_sem=send.at[d],
            recv_sem=recv.at[d],
            device_id={"sp": lax.rem(li + d, chain) * seqs + seq},
            device_id_type=MESH,
        )

    def r_copy(d):
        peer = lax.rem(tp + d, tps)
        return pltpu.make_async_remote_copy(
            src_ref=part.at[peer],
            dst_ref=landed.at[d],
            send_sem=r_send.at[d],
            recv_sem=r_recv.at[d],
            device_id={"tp": peer},
            device_id_type=MESH,
        )

    for d in range(1, tps):
        x_copy(d).start()
    pulls[0].wait()
    pulls[1].wait()

    def push_weights(d, _):
        for copy in w_copies(d):
            copy.start()
        return 0

    early = min(EARLY + 1, slots)
    lax.fori_loop(1, early, push_weights, 0)

    spread = (iota((per, chans), 1) % per == iota((per, chans), 0)).astype(F32)
    in_keep = (iota((flat, chans), 0) // states) == (iota((flat, chans), 1) // per)
    out_keep = (iota((chans, flat), 0) // per) == (iota((chans, flat), 1) // states)
    decay = params[0:1, :]
    lane = iota((rows, 2 * states), 1)
    pieces = [
        jnp.where(lane < states, extra[:, g : g + 1], extra[:, g + 1 : g + 2])
        for g in range(0, groups, 2)
    ]
    magnitude = jnp.exp(jnp.concatenate(pieces, axis=1) - decay)
    tr[...] = magnitude * params[1:2, :]
    ti[...] = magnitude * params[2:3, :]

    for d in range(1, tps):
        x_arrival(d).wait_recv()
    for pull in pulls[2:]:
        pull.wait()
    x = xall[...].reshape(rows, width)

    def turned(raw):
        tiles = []
        half = QK_DIM // 2
        first = (iota((rows, 128), 1) % QK_DIM) < half
        for c in range(0, raw.shape[1], 128):
            v = raw[:, c : c + 128]
            other = jnp.where(first, pltpu.roll(v, 128 - half, 1), pltpu.roll(v, half, 1))
            tiles.append(v * table[:, :128] + other * table[:, 128:])
        return tiles

    for i, tile in enumerate(turned(dot(x, wk[...]))):
        kv[0, :, i * 128 : (i + 1) * 128] = tile.astype(BF16)
    kv[0, :, qw:] = dot(x, wv[...]).astype(BF16)
    drive = dot(x, wd[...]).astype(BF16).astype(F32)

    def push_kv(d, _):
        @pl.when(li + d < chain)
        def _():
            chain_copy(kv, k_send, k_recv, d).start()

        return 0

    lax.fori_loop(1, chain, push_kv, 0)

    for which, ref in enumerate((ir, ii)):
        block = dot(in_map[which * flat : (which + 1) * flat, :], spread, HIGHEST)
        block = jnp.where(in_keep, block, 0.0)
        ref[...] = params[3:4, :] * dot_t(drive, block, HIGHEST)

    def scan_tile(i, carry):
        mr, mi, ar, ai = carry
        at = pl.ds(pl.multiple_of(i * 8, 8), 8)
        a, b, u, v = tr[at, :], ti[at, :], ir[at, :], ii[at, :]
        rows_out = ([], [], [], [])
        for r in range(8):
            p, q = a[r : r + 1], b[r : r + 1]
            mr, mi = p * mr - q * mi, p * mi + q * mr
            ar, ai = (
                p * ar - q * ai + u[r : r + 1],
                p * ai + q * ar + v[r : r + 1],
            )
            for keep, value in zip(rows_out, (mr, mi, ar, ai)):
                keep.append(value)
        for ref, keep in zip((tr, ti, ir, ii), rows_out):
            ref[at, :] = jnp.concatenate(keep, axis=0)
        return mr, mi, ar, ai

    one, zero = jnp.ones((1, flat), F32), jnp.zeros((1, flat), F32)
    mr, mi, ar, ai = lax.fori_loop(0, rows // 8, scan_tile, (one, zero, zero, zero))
    start_r, start_i = params[4:5, :], params[5:6, :]
    head_of_chain = li == 0
    entry_r = mr * start_r - mi * start_i + ar
    entry_i = mr * start_i + mi * start_r + ai
    summary[0] = jnp.concatenate(
        (
            jnp.where(head_of_chain, 0.0, mr),
            jnp.where(head_of_chain, 0.0, mi),
            jnp.where(head_of_chain, entry_r, ar),
            jnp.where(head_of_chain, entry_i, ai),
            zero,
            zero,
            zero,
            zero,
        ),
        axis=0,
    )

    q_tiles = turned(dot(x, wq[...]))
    low = iota((rows, 128), 1) < QK_DIM
    for h in range(heads):
        tile = q_tiles[h].astype(BF16).astype(F32) * QK_DIM**-0.5
        qz[2 * h] = jnp.where(low, tile, 0.0).astype(BF16)
        qz[2 * h + 1] = jnp.where(low, 0.0, tile).astype(BF16)

    def push_summary(d, _):
        @pl.when(li + d < chain)
        def _():
            chain_copy(summary, s_send, s_recv, d).start()

        return 0

    lax.fori_loop(1, chain, push_summary, 0)
    lax.fori_loop(early, slots, push_weights, 0)

    allowed = (iota((rows, rows), 1) // SEGMENT) <= (iota((rows, rows), 0) // SEGMENT)
    for u in range(2 * heads):
        h = u // 2
        s = dot_t(qz[u], kv[0, :, h * 128 : (h + 1) * 128])
        s = jnp.where(allowed, s, MASK_FLOOR)
        m = jnp.max(s, axis=-1, keepdims=True)
        e = jnp.where(allowed, jnp.exp(s - m), 0.0)
        peak[u] = jnp.broadcast_to(m, (rows, V_DIM))
        total[u] = jnp.broadcast_to(jnp.sum(e, axis=-1, keepdims=True), (rows, V_DIM))
        numer[u] = dot(e.astype(BF16), kv[0, :, qw + h * V_DIM : qw + (h + 1) * V_DIM])

    def earlier(j, _):
        @pl.when(j <= li)
        def _():
            chain_copy(kv, k_send, k_recv, j).wait_recv()
            for u in range(2 * heads):
                h = u // 2
                s = dot_t(qz[u], kv[j, :, h * 128 : (h + 1) * 128])
                before = peak[u]
                m = jnp.maximum(before, jnp.max(s, axis=-1, keepdims=True))
                shrink = jnp.exp(before - m)
                e = jnp.exp(s - m[:, :1])
                peak[u] = m
                total[u] = total[u] * shrink + jnp.sum(e, axis=-1, keepdims=True)
                numer[u] = numer[u] * shrink + dot(
                    e.astype(BF16), kv[j, :, qw + h * V_DIM : qw + (h + 1) * V_DIM]
                )

        return 0

    lax.fori_loop(1, chain, earlier, 0)

    for h in range(heads):
        diff = numer[2 * h] / total[2 * h] - mix[h] * (numer[2 * h + 1] / total[2 * h + 1])
        scale = lax.rsqrt(jnp.mean(diff * diff, axis=-1, keepdims=True) + EPSILON)
        acts[:, chans + h * V_DIM : chans + (h + 1) * V_DIM] = (
            diff * scale * sub_gain[...] * (1.0 - LAMBDA_INIT)
        ).astype(BF16)

    def enter(step, carry):
        j = chain - step

        def taken(carry):
            cr, ci = carry
            block = summary[j]
            a, b = block[0:1], block[1:2]
            return a * cr - b * ci + block[2:3], a * ci + b * cr + block[3:4]

        @pl.when(j <= li)
        def _():
            chain_copy(summary, s_send, s_recv, j).wait_recv()

        @pl.when(j > li)
        def _():
            summary[j] = jnp.zeros_like(summary[j])

        return taken(carry)

    cr, ci = lax.fori_loop(1, chain, enter, (zero, zero))
    cr = jnp.where(head_of_chain, start_r, cr)
    ci = jnp.where(head_of_chain, start_i, ci)
    state_r = tr[...] * cr - ti[...] * ci + ir[...]
    state_i = tr[...] * ci + ti[...] * cr + ii[...]
    blocks = [
        jnp.where(
            out_keep,
            jnp.concatenate([out_map[w * chans : (w + 1) * chans, :]] * groups, axis=1),
            0.0,
        )
        for w in range(2)
    ]
    mixed = dot_t(state_r, blocks[0], HIGHEST) - dot_t(state_i, blocks[1], HIGHEST)
    acts[:, :chans] = jax.nn.gelu(mixed + skip[...] * drive).astype(BF16)

    def project(j, _):
        if slots > 1:

            @pl.when(j > 0)
            def _():
                for copy in w_copies(j):
                    copy.wait_recv()

        block = dot(acts[:, :chans], wos[j]) + dot(acts[:, chans:], woa[j])
        at = pl.multiple_of(lax.rem(sp + slots - j, slots) * cols, 128)
        part[:, :, pl.ds(at, cols)] = block.astype(BF16).reshape(tps, own, cols)
        return 0

    lax.fori_loop(0, slots, project, 0)
    for d in range(1, tps):
        r_copy(d).start()
    summed = part[tp].astype(F32)
    for d in range(1, tps):
        r_copy(d).wait_recv()
        summed = summed + landed[d].astype(F32)
    out[...] = summed.astype(BF16)

    for d in range(1, tps):
        x_copy(d).wait_send()
        r_copy(d).wait_send()

    def drain(d, _):
        @pl.when(li + d < chain)
        def _():
            chain_copy(kv, k_send, k_recv, d).wait_send()
            chain_copy(summary, s_send, s_recv, d).wait_send()

        return 0

    lax.fori_loop(1, chain, drain, 0)

    def drain_weights(d, _):
        for copy in w_copies(d):
            copy.wait_send()
        return 0

    lax.fori_loop(1, slots, drain_weights, 0)


def local(
    mesh_shape,
    tokens,
    norm_gain,
    w_query,
    w_key,
    w_value,
    w_state_in,
    decay_rate,
    rotation,
    extra_decay,
    in_map,
    out_map,
    skip_gain,
    init_state,
    mix_lambda,
    sub_gain,
    w_out_state,
    w_out_attn,
):
    sps, tps = mesh_shape
    seqs = init_state.shape[0]
    chain = sps // seqs
    own, width = tokens.shape
    rows = own * tps
    if rows % SEGMENT:
        raise ValueError("rows")
    groups, states = decay_rate.shape
    flat = groups * states
    chans = w_state_in.shape[1]
    qw = w_query.shape[1]
    vw = w_value.shape[1]
    units = 2 * vw // V_DIM
    sp = lax.axis_index("sp")
    if seqs == 1 and w_out_state.shape[1] % 128 == 0:
        slots = sps
    else:
        slots = 1
        w_out_state = lax.all_gather(w_out_state, "sp", axis=1, tiled=True)
        w_out_attn = lax.all_gather(w_out_attn, "sp", axis=1, tiled=True)
    cols = w_out_state.shape[1]

    half = QK_DIM // 2
    inverse = ROTARY_BASE ** (-2.0 * jnp.arange(half, dtype=F32) / QK_DIM)
    positions = ((sp // seqs) * rows + jnp.arange(rows, dtype=jnp.int32)).astype(F32)
    angles = positions[:, None] * inverse[None, :]
    cosine, sine = jnp.cos(angles), jnp.sin(angles)
    copies = 128 // QK_DIM
    table = jnp.concatenate((cosine, cosine) * copies + (-sine, sine) * copies, axis=1)

    start = lax.dynamic_index_in_dim(init_state, sp % seqs, 0, keepdims=False)
    zero = jnp.zeros((1, flat), F32)
    params = jnp.concatenate(
        (
            decay_rate.reshape(1, flat),
            jnp.cos(rotation).reshape(1, flat),
            jnp.sin(rotation).reshape(1, flat),
            jnp.sqrt(-jnp.expm1(-2.0 * decay_rate)).reshape(1, flat),
            start.reshape(2, flat),
            zero,
            zero,
        ),
        axis=0,
    )

    vmem = pl.BlockSpec(memory_space=pltpu.VMEM)
    hbm = pl.BlockSpec(memory_space=pl.ANY)
    smem = pl.BlockSpec(memory_space=pltpu.SMEM)
    dma = pltpu.SemaphoreType.DMA
    return pl.pallas_call(
        functools.partial(kernel, (seqs, chain, tps, slots)),
        out_shape=jax.ShapeDtypeStruct((own, width), BF16),
        in_specs=[vmem, vmem, hbm, hbm, hbm, hbm]
        + [vmem] * 6
        + [smem, vmem, hbm, hbm],
        out_specs=vmem,
        scratch_shapes=[
            pltpu.VMEM((tps, own, width), BF16),
            pltpu.VMEM(w_query.shape, BF16),
            pltpu.VMEM(w_key.shape, BF16),
            pltpu.VMEM(w_value.shape, BF16),
            pltpu.VMEM(w_state_in.shape, BF16),
            pltpu.VMEM((slots,) + w_out_state.shape, BF16),
            pltpu.VMEM((slots,) + w_out_attn.shape, BF16),
            pltpu.VMEM((units, rows, 128), BF16),
            pltpu.VMEM((chain, rows, qw + vw), BF16),
            pltpu.VMEM((chain, 8, flat), F32),
            pltpu.VMEM((rows, flat), F32),
            pltpu.VMEM((rows, flat), F32),
            pltpu.VMEM((rows, flat), F32),
            pltpu.VMEM((rows, flat), F32),
            pltpu.VMEM((units, rows, V_DIM), F32),
            pltpu.VMEM((units, rows, V_DIM), F32),
            pltpu.VMEM((units, rows, V_DIM), F32),
            pltpu.VMEM((tps, own, width), BF16),
            pltpu.VMEM((tps, own, width), BF16),
            pltpu.VMEM((rows, chans + vw), BF16),
            dma((6,)),
            dma((tps,)),
            dma((tps,)),
            dma((2, slots)),
            dma((2, slots)),
            dma((chain,)),
            dma((chain,)),
            dma((chain,)),
            dma((chain,)),
            dma((tps,)),
            dma((tps,)),
        ],
        compiler_params=pltpu.CompilerParams(
            collective_id=0, has_side_effects=True, vmem_limit_bytes=48 * 1024 * 1024
        ),
    )(
        tokens,
        norm_gain.reshape(1, width),
        w_query,
        w_key,
        w_value,
        w_state_in,
        table,
        params,
        extra_decay,
        in_map.reshape(2 * flat, chans // groups),
        out_map.reshape(2 * chans, states),
        skip_gain.reshape(1, chans),
        mix_lambda,
        sub_gain.reshape(1, V_DIM),
        w_out_state,
        w_out_attn,
    )


def solution(mesh):
    in_specs = (
        P(("sp", "tp"), None),
        P(),
        P(None, "tp"),
        P(None, "tp"),
        P(None, "tp"),
        P(None, "tp"),
        P("tp", None),
        P("tp", None),
        P("sp", "tp"),
        P(None, "tp", None, None),
        P(None, "tp", None, None),
        P("tp", None),
        P(None, None, "tp", None),
        P("tp"),
        P(),
        P("tp", "sp"),
        P("tp", "sp"),
    )
    shape = (mesh.shape["sp"], mesh.shape["tp"])
    return jax.shard_map(
        functools.partial(local, shape),
        mesh=mesh,
        in_specs=in_specs,
        out_specs=P(("sp", "tp"), None),
        check_vma=False,
    )
```

profile of v0, /device:TPU:29, one launch (start us, length us, event | category | flops | bytes accessed | tf_op | source)
XLA Modules:
  0.0 88.9 jit_solution(13127538480067978249)
XLA Ops:
  0.0 0.0 copy-start
  0.0 0.9 reshape.49.skip
  0.9 0.8 reshape.42
  1.6 0.8 reshape.46
  2.4 0.7 negate_sqrt_fusion
  3.1 0.1 reshape.45
  3.2 0.7 fusion.1
  3.9 0.1 reshape.44
  4.0 0.1 reshape.43
  4.1 0.8 copy.22.extra
  4.9 0.3 multiply_sine_fusion
  5.2 0.0 copy-start.3
  5.2 0.2 concatenate.9.table
  5.4 0.0 copy-start.4
  5.4 1.1 %copy.21 = f32[2,8,64,16]{3,2,1,0:T(8,128)S(1)} copy(f32[2,8,64,16]{2,3,1,0:T(8,128)} %param.26) | data formatting | bytes 131072 | tf_op args[9]
  6.6 0.0 copy-start.9
  6.6 0.0 copy-start.10
  6.6 0.0 copy-done
  6.6 0.0 copy-done.3
  6.6 0.0 copy-done.4
  6.6 0.6 copy-done.9
  7.2 0.0 copy-done.10
  7.3 0.0 copy-start.1
  7.3 1.2 %copy-done.1 = bf16[2048,256]{1,0:T(8,128)(2,1)S(1)} copy-done((bf16[2048,256]{1,0:T(8,128)(2,1)S(1)}, bf16[2048,256]{1,0:T(8,128)(2,1)}, u32[]{:S(2)}) %copy-start.1) | copy-done | bytes 1048600
  8.5 0.0 copy-start.2
  8.5 1.2 %copy-done.2 = bf16[2048,256]{1,0:T(8,128)(2,1)S(1)} copy-done((bf16[2048,256]{1,0:T(8,128)(2,1)S(1)}, bf16[2048,256]{1,0:T(8,128)(2,1)}, u32[]{:S(2)}) %copy-start.2) | copy-done | bytes 1048600
  9.7 0.0 copy-start.5
  9.7 0.9 %copy-done.5 = f32[2,8,16,64]{3,2,1,0:T(8,128)S(1)} copy-done((f32[2,8,16,64]{3,2,1,0:T(8,128)S(1)}, f32[2,8,16,64]{3,2,1,0:T(8,128)}, u32[]{:S(2)}) %copy-start.5) | copy-done | bytes 65560
  10.6 0.0 copy-start.6
  10.6 0.9 %copy-done.6 = bf16[256,256]{1,0:T(8,128)(2,1)S(1)} copy-done((bf16[256,256]{1,0:T(8,128)(2,1)S(1)}, bf16[256,256]{1,0:T(8,128)(2,1)}, u32[]{:S(2)}) %copy-start.6) | copy-done | bytes 131096
  11.5 0.0 copy-start.7
  11.5 0.8 copy-done.7
  12.4 0.0 copy-start.8
  12.4 0.7 copy-done.8
  13.1 75.2 %shard_map.163 = bf16[32,2048]{1,0:T(8,128)(2,1)S(1)} custom-call(bf16[32,2048]{1,0:T(8,128)(2,1)S(1)} %copy-done.4, f32[1,2048]{1,0:T(1,128)S(1)} %bitcast.8, bf16[2048,256]{1,0:T(8,128)(2,1)S(1)} %copy-done, bf16[2048,256]{1,0:T(8,128)(2,1)S(1)} %copy-done.1, bf16[2048,256]{1,0:T(8,128)(2,1)S(1)} %copy-done.2, bf16[2048,128]{1,0:T(8,128)(2,1)S(1)} %copy-done.3, ...), custom_call_target="tpu_custom_call" | custom-call | tf_op jit(solution)/shard_map/pallas_call | solution.py:506
  88.2 0.7 copy.24
  (4 shorter events, 0.0 us)
Async XLA Ops:
  0.0 6.6 %copy-start = (bf16[2048,256]{1,0:T(8,128)(2,1)S(1)}, bf16[2048,256]{1,0:T(8,128)(2,1)}, u32[]{:S(2)}) copy-start(bf16[2048,256]{1,0:T(8,128)(2,1)} %wq_hbm.1) | copy-start | bytes 3145732
  5.2 1.4 %copy-start.3 = (bf16[2048,128]{1,0:T(8,128)(2,1)S(1)}, bf16[2048,128]{1,0:T(8,128)(2,1)}, u32[]{:S(2)}) copy-start(bf16[2048,128]{1,0:T(8,128)(2,1)} %wd_hbm.1) | copy-start | bytes 1572868
  5.4 1.2 %copy-start.4 = (bf16[32,2048]{1,0:T(8,128)(2,1)S(1)}, bf16[32,2048]{1,0:T(8,128)(2,1)}, u32[]{:S(2)}) copy-start(bf16[32,2048]{1,0:T(8,128)(2,1)} %tokens.1) | copy-start | bytes 393220
  6.6 0.7 copy-start.9
  6.6 0.7 copy-start.10
  7.3 1.2 %copy-start.1 = (bf16[2048,256]{1,0:T(8,128)(2,1)S(1)}, bf16[2048,256]{1,0:T(8,128)(2,1)}, u32[]{:S(2)}) copy-start(bf16[2048,256]{1,0:T(8,128)(2,1)} %wk_hbm.1) | copy-start | bytes 3145732
  8.5 1.2 %copy-start.2 = (bf16[2048,256]{1,0:T(8,128)(2,1)S(1)}, bf16[2048,256]{1,0:T(8,128)(2,1)}, u32[]{:S(2)}) copy-start(bf16[2048,256]{1,0:T(8,128)(2,1)} %wv_hbm.1) | copy-start | bytes 3145732
  9.7 0.9 %copy-start.5 = (f32[2,8,16,64]{3,2,1,0:T(8,128)S(1)}, f32[2,8,16,64]{3,2,1,0:T(8,128)}, u32[]{:S(2)}) copy-start(f32[2,8,16,64]{3,2,1,0:T(8,128)} %param.27) | copy-start | bytes 196612
  10.6 0.9 %copy-start.6 = (bf16[256,256]{1,0:T(8,128)(2,1)S(1)}, bf16[256,256]{1,0:T(8,128)(2,1)}, u32[]{:S(2)}) copy-start(bf16[256,256]{1,0:T(8,128)(2,1)} %wa_hbm.1) | copy-start | bytes 393220
  11.5 0.8 copy-start.7
  12.4 0.7 copy-start.8
where the time goes:
time: 89.4 us; the launch traced here: 88.9 us
  Pallas kernels  75.2 us (84%)
  local copies, waits for them, and re-layouts  12.6 us (14%)
  other arithmetic  1.02 us (1%)
    pallas_call x1, Pallas kernels, local(): pl.pallas_call(functools.partial(kernel, (seqs, chain, tps, slots)), out_...  75.2 us
    unnamed x25, local copies, waits for them, and re-layouts  9.03 us

commit v1 on v0

v1 whole, which is shorter than its diff:
```python
import functools
import math

import jax
import jax.numpy as jnp
from jax import lax
from jax.experimental import pallas as pl
from jax.experimental.pallas import tpu as pltpu
from jax.sharding import PartitionSpec as P

QK_DIM = 64
V_DIM = 128
SEGMENT = 64
EPSILON = 1e-06
ROTARY_BASE = 10000.0
LAMBDA_INIT = 0.2
MASK_FLOOR = -1e30
F32 = jnp.float32
BF16 = jnp.bfloat16
MESH = pl.DeviceIdType.MESH
HIGHEST = lax.Precision.HIGHEST


def dot(a, b, precision=None):
    return jnp.dot(a, b, preferred_element_type=F32, precision=precision)


def dot_t(a, b, precision=None):
    return lax.dot_general(
        a, b, (((1,), (1,)), ((), ())), preferred_element_type=F32, precision=precision
    )


def one_less_exp(x):
    series = jnp.ones_like(x)
    for n in range(9, 1, -1):
        series = 1.0 - x * series * (1.0 / n)
    return jnp.where(x < 0.5, x * series, 1.0 - jnp.exp(-x))


def iota(shape, axis):
    return lax.broadcasted_iota(jnp.int32, shape, axis)


def kernel(
    cfg,
    tokens,
    gain,
    wq_hbm,
    wk_hbm,
    wv_hbm,
    wd_hbm,
    decay_in,
    turn_in,
    start_in,
    extra_t,
    in_map,
    out_map,
    skip,
    mix,
    sub_gain,
    ws_hbm,
    wa_hbm,
    out,
    xall,
    wq,
    wk,
    wv,
    wd,
    wo,
    qz,
    kv,
    summary,
    tr,
    ti,
    ir,
    ii,
    peak,
    total,
    numer,
    part,
    landed,
    acts,
    local_sem,
    x_send,
    x_recv,
    wu_send,
    wd_send,
    wy_send,
    wz_recv,
    wy_recv,
    ku_send,
    ky_send,
    kz_recv,
    ky_recv,
    s_send,
    s_recv,
    r_send,
    r_recv,
):
    seqs, chain, tps, fold, gather = cfg
    reach = chain // fold
    sp = lax.axis_index("sp")
    tp = lax.axis_index("tp")
    li = sp // seqs
    seq = sp % seqs
    zi, yi = li // fold, li % fold
    own, width = tokens.shape
    rows = own * tps
    heads = wv.shape[1] // V_DIM
    qw = wq.shape[1]
    cols = wo.shape[3]
    flat = tr.shape[1]
    groups = extra_t.shape[0]
    states = flat // groups
    chans = wd.shape[1]
    per = chans // groups

    pulls = [
        pltpu.make_async_copy(src, dst, local_sem.at[i])
        for i, (src, dst) in enumerate(
            (
                (ws_hbm, wo.at[0, 0, pl.ds(0, chans)]),
                (wa_hbm, wo.at[0, 0, pl.ds(chans, wa_hbm.shape[0])]),
                (wd_hbm, wd),
                (wk_hbm, wk),
                (wv_hbm, wv),
                (wq_hbm, wq),
            )
        )
    ]
    for pull in pulls:
        pull.start()

    barrier = pltpu.get_barrier_semaphore()

    def greet_tp(d, _):
        pl.semaphore_signal(
            barrier, inc=1, device_id={"tp": lax.rem(tp + d, tps)}, device_id_type=MESH
        )
        return 0

    def greet_sp(d, _):
        pl.semaphore_signal(
            barrier,
            inc=1,
            device_id={"sp": lax.rem(li + d, chain) * seqs + seq},
            device_id_type=MESH,
        )
        return 0

    lax.fori_loop(1, tps, greet_tp, 0)
    lax.fori_loop(1, chain, greet_sp, 0)

    wide = tokens[...].astype(F32)
    scale = lax.rsqrt(jnp.mean(wide * wide, axis=-1, keepdims=True) + EPSILON)
    xall[tp] = (wide * scale * gain[...]).astype(BF16)

    pl.semaphore_wait(barrier, tps - 1 + chain - 1)

    def send(src, dst, send_sem, recv_sem, device_id):
        return pltpu.make_async_remote_copy(
            src_ref=src,
            dst_ref=dst,
            send_sem=send_sem,
            recv_sem=recv_sem,
            device_id=device_id,
            device_id_type=MESH,
        )

    def at_chain(z, y):
        return {"sp": (z * fold + y) * seqs + seq}

    above = at_chain(lax.rem(zi + 1, reach), yi)
    below = at_chain(lax.rem(zi + reach - 1, reach), yi)
    across = at_chain(zi, fold - 1 - yi)

    def tp_peer(d):
        return tp + d - 2 * d * ((tp // d) % 2)

    def x_copy(d):
        if tps == 4:
            row = tp_peer(2) if d == 3 else tp
            peer = tp_peer(2) if d == 2 else tp_peer(1)
        else:
            row, peer = tp, lax.rem(tp + d, tps)
        return send(xall.at[row], xall.at[row], x_send.at[d], x_recv.at[d], {"tp": peer})

    def x_wait(d):
        if tps == 4:
            row = tps - 1 - tp if d == 3 else tp_peer(d)
        else:
            row = lax.rem(tp + tps - d, tps)
        peer = {"tp": lax.rem(tp + 1, tps)}
        send(xall.at[tp], xall.at[row], x_send.at[d], x_recv.at[d], peer).wait_recv()

    def w_up(k):
        src, dst = (reach - k) % reach, reach - k - 1
        return send(wo.at[src, 0], wo.at[dst, 0], wu_send.at[k], wz_recv.at[dst], above)

    def w_down(k):
        return send(wo.at[k, 0], wo.at[k + 1, 0], wd_send.at[k], wz_recv.at[k + 1], below)

    def w_across(r):
        return send(wo.at[r, 0], wo.at[r, 1], wy_send.at[r], wy_recv.at[r], across)

    def w_arrived(r):
        send(wo.at[r, 0], wo.at[r, 0], wy_send.at[r], wz_recv.at[r], above).wait_recv()

    def w_own():
        @pl.when(zi + 1 < reach)
        def _():
            w_up(0).start()

        @pl.when(zi >= 1)
        def _():
            w_down(0).start()

        if fold == 2:
            w_across(0).start()

    def w_relay(k):
        for there, r in ((zi >= k, reach - k), (zi + k < reach, k)):

            @pl.when(there)
            def _():
                w_arrived(r)

        if k + 1 < reach:

            @pl.when((zi >= k) & (zi + 1 < reach))
            def _():
                w_up(k).start()

            @pl.when((zi + k < reach) & (zi >= 1))
            def _():
                w_down(k).start()

        if fold == 2:
            for there, r in ((zi >= k, reach - k), (zi + k < reach, k)):

                @pl.when(there)
                def _():
                    w_across(r).start()

    def k_up(k):
        return send(kv.at[k, 0], kv.at[k + 1, 0], ku_send.at[k], kz_recv.at[k + 1], above)

    def k_across(k):
        return send(kv.at[k, 0], kv.at[k, 1], ky_send.at[k], ky_recv.at[k], across)

    def k_arrived(k):
        send(kv.at[k, 0], kv.at[k, 0], ky_send.at[k], kz_recv.at[k], above).wait_recv()

    def summary_copy(d):
        return send(
            summary.at[0],
            summary.at[d],
            s_send.at[d],
            s_recv.at[d],
            {"sp": lax.rem(li + d, chain) * seqs + seq},
        )

    def r_copy(slot, d, at):
        peer = lax.rem(tp + d, tps)
        return send(
            part.at[peer, :, pl.ds(at, cols)],
            landed.at[d, :, pl.ds(at, cols)],
            r_send.at[slot, d],
            r_recv.at[slot, d],
            {"tp": peer},
        )

    if tps == 4:
        x_copy(2).start()
        x_copy(1).start()
    else:
        for d in range(1, tps):
            x_copy(d).start()
    pulls[0].wait()
    pulls[1].wait()
    if gather:
        w_own()

    inner = iota((rows, 128), 1) % QK_DIM
    half = QK_DIM // 2
    power = (inner % half).astype(F32) * (-2.0 / QK_DIM)
    angle = (li * rows + iota((rows, 128), 0)).astype(F32) * jnp.exp(
        power * math.log(ROTARY_BASE)
    )
    cosine = jnp.cos(angle)
    sine = jnp.sin(angle)
    sine = jnp.where(inner < half, -sine, sine)

    def level(ref, first, count):
        return jnp.concatenate([ref[g : g + 1, :] for g in range(first, first + count)], axis=1)

    decay = level(decay_in, 0, groups)
    turn = level(turn_in, 0, groups)
    start_r, start_i = level(start_in, 0, groups), level(start_in, groups, groups)
    in_scale = jnp.sqrt(one_less_exp(2.0 * decay))
    straight = level(skip, 0, groups)

    keep = (iota((chans, flat), 0) // per) == (iota((chans, flat), 1) // states)

    def block_map(ref, which):
        tall = ref[which * chans : (which + 1) * chans, :]
        return jnp.where(keep, jnp.concatenate([tall] * groups, axis=1), 0.0)

    extra = extra_t[...].T
    lane = iota((rows, 2 * states), 1)
    pieces = [
        jnp.where(lane < states, extra[:, g : g + 1], extra[:, g + 1 : g + 2])
        for g in range(0, groups, 2)
    ]
    magnitude = jnp.exp(jnp.concatenate(pieces, axis=1) - decay)
    tr[...] = magnitude * jnp.cos(turn)
    ti[...] = magnitude * jnp.sin(turn)

    if tps == 4:
        x_wait(2)
        x_copy(3).start()
    for d in range(1, tps):
        if d != 2 or tps != 4:
            x_wait(d)
    for pull in pulls[2:]:
        pull.wait()
    x = xall[...].reshape(rows, width)

    def turned(raw):
        tiles = []
        first = inner < half
        for c in range(0, raw.shape[1], 128):
            v = raw[:, c : c + 128]
            other = jnp.where(first, pltpu.roll(v, 128 - half, 1), pltpu.roll(v, half, 1))
            tiles.append(v * cosine + other * sine)
        return tiles

    for i, tile in enumerate(turned(dot(x, wk[...]))):
        kv[0, 0, :, i * 128 : (i + 1) * 128] = tile.astype(BF16)
    kv[0, 0, :, qw:] = dot(x, wv[...]).astype(BF16)
    drive = dot(x, wd[...]).astype(BF16).astype(F32)

    @pl.when(zi + 1 < reach)
    def _():
        k_up(0).start()

    if fold == 2:

        @pl.when(yi == 0)
        def _():
            k_across(0).start()

    if gather and reach > 1:
        w_relay(1)

    for which, ref in enumerate((ir, ii)):
        ref[...] = in_scale * dot(drive, block_map(in_map, which), HIGHEST)

    def scan_tile(i, carry):
        mr, mi, ar, ai = carry
        at = pl.ds(pl.multiple_of(i * 8, 8), 8)
        a, b, u, v = tr[at, :], ti[at, :], ir[at, :], ii[at, :]
        rows_out = ([], [], [], [])
        for r in range(8):
            p, q = a[r : r + 1], b[r : r + 1]
            mr, mi = p * mr - q * mi, p * mi + q * mr
            ar, ai = (
                p * ar - q * ai + u[r : r + 1],
                p * ai + q * ar + v[r : r + 1],
            )
            for keep, value in zip(rows_out, (mr, mi, ar, ai)):
                keep.append(value)
        for ref, keep in zip((tr, ti, ir, ii), rows_out):
            ref[at, :] = jnp.concatenate(keep, axis=0)
        return mr, mi, ar, ai

    one, zero = jnp.ones((1, flat), F32), jnp.zeros((1, flat), F32)
    mr, mi, ar, ai = lax.fori_loop(0, rows // 8, scan_tile, (one, zero, zero, zero))
    head_of_chain = li == 0
    entry_r = mr * start_r - mi * start_i + ar
    entry_i = mr * start_i + mi * start_r + ai
    summary[0] = jnp.concatenate(
        (
            jnp.where(head_of_chain, 0.0, mr),
            jnp.where(head_of_chain, 0.0, mi),
            jnp.where(head_of_chain, entry_r, ar),
            jnp.where(head_of_chain, entry_i, ai),
            zero,
            zero,
            zero,
            zero,
        ),
        axis=0,
    )

    q_tiles = turned(dot(x, wq[...]))
    low = iota((rows, 128), 1) < QK_DIM
    for h in range(heads):
        tile = q_tiles[h].astype(BF16).astype(F32) * QK_DIM**-0.5
        qz[2 * h] = jnp.where(low, tile, 0.0).astype(BF16)
        qz[2 * h + 1] = jnp.where(low, 0.0, tile).astype(BF16)

    def push_summary(d, _):
        @pl.when(li + d < chain)
        def _():
            summary_copy(d).start()

        return 0

    lax.fori_loop(1, chain, push_summary, 0)

    def relay_kv(k):
        @pl.when(zi >= k)
        def _():
            k_arrived(k)
            if k + 1 < reach:

                @pl.when(zi + 1 < reach)
                def _():
                    k_up(k).start()

            if fold == 2:
                k_across(k).start()

    allowed = (iota((rows, rows), 1) // SEGMENT) <= (iota((rows, rows), 0) // SEGMENT)
    for u in range(2 * heads):
        h = u // 2
        s = dot_t(qz[u], kv[0, 0, :, h * 128 : (h + 1) * 128])
        s = jnp.where(allowed, s, MASK_FLOOR)
        m = jnp.max(s, axis=-1, keepdims=True)
        e = jnp.where(allowed, jnp.exp(s - m), 0.0)
        peak[u] = jnp.broadcast_to(m, (rows, V_DIM))
        total[u] = jnp.broadcast_to(jnp.sum(e, axis=-1, keepdims=True), (rows, V_DIM))
        numer[u] = dot(e.astype(BF16), kv[0, 0, :, qw + h * V_DIM : qw + (h + 1) * V_DIM])

    def attend(k, c):
        for u in range(2 * heads):
            h = u // 2
            s = dot_t(qz[u], kv[k, c, :, h * 128 : (h + 1) * 128])
            before = peak[u]
            m = jnp.maximum(before, jnp.max(s, axis=-1, keepdims=True))
            shrink = jnp.exp(before - m)
            e = jnp.exp(s - m[:, :1])
            peak[u] = m
            total[u] = total[u] * shrink + jnp.sum(e, axis=-1, keepdims=True)
            numer[u] = numer[u] * shrink + dot(
                e.astype(BF16), kv[k, c, :, qw + h * V_DIM : qw + (h + 1) * V_DIM]
            )

    def attend_across(k, there):
        @pl.when(there)
        def _():
            k_across(k).wait_recv()
            attend(k, 1)

    for k in range(1, reach):
        relay_kv(k)
        if gather and k >= 2:
            w_relay(k)
        if fold == 2:
            attend_across(k - 1, (zi >= k - 1) if k > 1 else (yi == 1))

        @pl.when(zi >= k)
        def _():
            attend(k, 0)

    if fold == 2:
        attend_across(reach - 1, (zi >= reach - 1) if reach > 1 else (yi == 1))

    for h in range(heads):
        diff = numer[2 * h] / total[2 * h] - mix[h] * (numer[2 * h + 1] / total[2 * h + 1])
        scale = lax.rsqrt(jnp.mean(diff * diff, axis=-1, keepdims=True) + EPSILON)
        acts[:, chans + h * V_DIM : chans + (h + 1) * V_DIM] = (
            diff * scale * sub_gain[...] * (1.0 - LAMBDA_INIT)
        ).astype(BF16)

    def enter(step, carry):
        j = chain - step

        def taken(carry):
            cr, ci = carry
            block = summary[j]
            a, b = block[0:1], block[1:2]
            return a * cr - b * ci + block[2:3], a * ci + b * cr + block[3:4]

        @pl.when(j <= li)
        def _():
            summary_copy(j).wait_recv()

        @pl.when(j > li)
        def _():
            summary[j] = jnp.zeros_like(summary[j])

        return taken(carry)

    cr, ci = lax.fori_loop(1, chain, enter, (zero, zero))
    cr = jnp.where(head_of_chain, start_r, cr)
    ci = jnp.where(head_of_chain, start_i, ci)
    state_r = tr[...] * cr - ti[...] * ci + ir[...]
    state_i = tr[...] * ci + ti[...] * cr + ii[...]
    blocks = [block_map(out_map, w) for w in range(2)]
    mixed = dot_t(state_r, blocks[0], HIGHEST) - dot_t(state_i, blocks[1], HIGHEST)
    acts[:, :chans] = jax.nn.gelu(mixed + straight * drive).astype(BF16)

    shares = [(r, c) for r in range(reach) for c in range(fold)] if gather else [(0, 0)]
    order = sorted(range(len(shares)), key=lambda i: min(shares[i][0], reach - shares[i][0]))

    def place(r, c):
        if not gather:
            return 0
        y = (yi + c) % fold
        return pl.multiple_of((lax.rem(zi + r, reach) * fold + y) * cols, 128)

    for i in order:
        r, c = shares[i]
        if c:
            w_across(r).wait_recv()
        block = dot(acts[...], wo[r, c])
        at = place(r, c)
        part[:, :, pl.ds(at, cols)] = block.astype(BF16).reshape(tps, own, cols)
        for d in range(1, tps):
            r_copy(i, d, at).start()
    summed = part[tp].astype(F32)
    for i in order:
        for d in range(1, tps):
            r_copy(i, d, place(*shares[i])).wait_recv()
    for d in range(1, tps):
        summed = summed + landed[d].astype(F32)
    out[...] = summed.astype(BF16)

    for d in range(1, tps):
        x_copy(d).wait_send()
        for i in order:
            r_copy(i, d, place(*shares[i])).wait_send()

    def drain(d, _):
        @pl.when(li + d < chain)
        def _():
            summary_copy(d).wait_send()

        return 0

    lax.fori_loop(1, chain, drain, 0)

    for k in range(reach):

        @pl.when((zi >= k) & (zi + 1 < reach))
        def _():
            if k + 1 < reach:
                k_up(k).wait_send()
                if gather:
                    w_up(k).wait_send()

        if gather:

            @pl.when((zi + k < reach) & (zi >= 1))
            def _():
                if k + 1 < reach:
                    w_down(k).wait_send()

        if fold == 2:

            @pl.when((zi >= k) if k else (yi == 0))
            def _():
                k_across(k).wait_send()

            if gather:
                w_across(k).wait_send()


def local(
    mesh_shape,
    tokens,
    norm_gain,
    w_query,
    w_key,
    w_value,
    w_state_in,
    decay_rate,
    rotation,
    extra_decay,
    in_map,
    out_map,
    skip_gain,
    init_state,
    mix_lambda,
    sub_gain,
    w_out_state,
    w_out_attn,
):
    sps, tps = mesh_shape
    seqs = init_state.shape[0]
    chain = sps // seqs
    own, width = tokens.shape
    rows = own * tps
    if rows % SEGMENT:
        raise ValueError("rows")
    groups, states = decay_rate.shape
    flat = groups * states
    chans = w_state_in.shape[1]
    qw = w_query.shape[1]
    vw = w_value.shape[1]
    units = 2 * vw // V_DIM
    sp = lax.axis_index("sp")
    fold = 2 if chain % 2 == 0 else 1
    reach = chain // fold
    gather = seqs == 1 and w_out_state.shape[1] % 128 == 0
    if not gather:
        w_out_state = lax.all_gather(w_out_state, "sp", axis=1, tiled=True)
        w_out_attn = lax.all_gather(w_out_attn, "sp", axis=1, tiled=True)
    cols = w_out_state.shape[1]
    shares = chain if gather else 1
    wo_shape = ((reach, fold) if gather else (1, 1)) + (chans + vw, cols)
    start = lax.dynamic_index_in_dim(init_state, sp % seqs, 0, keepdims=False)

    vmem = pl.BlockSpec(memory_space=pltpu.VMEM)
    hbm = pl.BlockSpec(memory_space=pl.ANY)
    smem = pl.BlockSpec(memory_space=pltpu.SMEM)
    dma = pltpu.SemaphoreType.DMA
    return pl.pallas_call(
        functools.partial(kernel, (seqs, chain, tps, fold, gather)),
        out_shape=jax.ShapeDtypeStruct((own, width), BF16),
        in_specs=[vmem, vmem, hbm, hbm, hbm, hbm]
        + [vmem] * 7
        + [smem, vmem, hbm, hbm],
        out_specs=vmem,
        scratch_shapes=[
            pltpu.VMEM((tps, own, width), BF16),
            pltpu.VMEM(w_query.shape, BF16),
            pltpu.VMEM(w_key.shape, BF16),
            pltpu.VMEM(w_value.shape, BF16),
            pltpu.VMEM(w_state_in.shape, BF16),
            pltpu.VMEM(wo_shape, BF16),
            pltpu.VMEM((units, rows, 128), BF16),
            pltpu.VMEM((reach, fold, rows, qw + vw), BF16),
            pltpu.VMEM((chain, 8, flat), F32),
            pltpu.VMEM((rows, flat), F32),
            pltpu.VMEM((rows, flat), F32),
            pltpu.VMEM((rows, flat), F32),
            pltpu.VMEM((rows, flat), F32),
            pltpu.VMEM((units, rows, V_DIM), F32),
            pltpu.VMEM((units, rows, V_DIM), F32),
            pltpu.VMEM((units, rows, V_DIM), F32),
            pltpu.VMEM((tps, own, width), BF16),
            pltpu.VMEM((tps, own, width), BF16),
            pltpu.VMEM((rows, chans + vw), BF16),
            dma((6,)),
            dma((tps,)),
            dma((tps,)),
            dma((reach,)),
            dma((reach,)),
            dma((reach,)),
            dma((reach,)),
            dma((reach,)),
            dma((reach,)),
            dma((reach,)),
            dma((reach,)),
            dma((reach,)),
            dma((chain,)),
            dma((chain,)),
            dma((shares, tps)),
            dma((shares, tps)),
        ],
        compiler_params=pltpu.CompilerParams(
            collective_id=0, has_side_effects=True, vmem_limit_bytes=67043328
        ),
    )(
        tokens,
        norm_gain.reshape(1, width),
        w_query,
        w_key,
        w_value,
        w_state_in,
        decay_rate,
        rotation,
        start.reshape(2 * groups, states),
        extra_decay.T,
        in_map.swapaxes(2, 3).reshape(2 * chans, states),
        out_map.reshape(2 * chans, states),
        skip_gain,
        mix_lambda,
        sub_gain.reshape(1, V_DIM),
        w_out_state,
        w_out_attn,
    )


def solution(mesh):
    in_specs = (
        P(("sp", "tp"), None),
        P(),
        P(None, "tp"),
        P(None, "tp"),
        P(None, "tp"),
        P(None, "tp"),
        P("tp", None),
        P("tp", None),
        P("sp", "tp"),
        P(None, "tp", None, None),
        P(None, "tp", None, None),
        P("tp", None),
        P(None, None, "tp", None),
        P("tp"),
        P(),
        P("tp", "sp"),
        P("tp", "sp"),
    )
    shape = (mesh.shape["sp"], mesh.shape["tp"])
    return jax.shard_map(
        functools.partial(local, shape),
        mesh=mesh,
        in_specs=in_specs,
        out_specs=P(("sp", "tp"), None),
        check_vma=False,
    )
```

time: 89.4 us -> 48.7 us (0.54)
  Pallas kernels: 75.2 us -> 46.4 us
  local copies, waits for them, and re-layouts: 12.6 us -> 1.57 us
  other arithmetic: 1.02 us -> 0 us
    pallas_call x1, Pallas kernels: 75.2 us -> 46.4 us  [local(): pl.pallas_call(functools.partial(kernel, (seqs, chain, tps, fold, gather)...]
    unnamed x25 -> x1, local copies, waits for them, and re-layouts: 9.03 us -> 1.57 us
    reshape x6 -> x0, local copies, waits for them, and re-layouts: 2.63 us -> none  [the longest x1 0.85 us: local(): skip_gain.reshape(1, chans)]
where the time goes in v1:
time: 48.7 us; the launch traced here: 48 us
  Pallas kernels  46.4 us (95%)
  local copies, waits for them, and re-layouts  1.57 us (3%)
    pallas_call x1, Pallas kernels, local(): pl.pallas_call(functools.partial(kernel, (seqs, chain, tps, fold, gather)...  46.4 us
    unnamed x1, local copies, waits for them, and re-layouts  1.57 us

profile of v1, /device:TPU:29, one launch (start us, length us, event | category | flops | bytes accessed | tf_op | source)
XLA Modules:
  0.0 48.0 jit_solution(6402765864999067521)
XLA Ops:
  0.0 46.4 %shard_map.163 = bf16[32,2048]{1,0:T(8,128)(2,1)} custom-call(bf16[32,2048]{1,0:T(8,128)(2,1)} %tokens.1, f32[1,2048]{1,0:T(1,128)} %bitcast.10, bf16[2048,256]{1,0:T(8,128)(2,1)} %wq_hbm.1, bf16[2048,256]{1,0:T(8,128)(2,1)} %wk_hbm.1, bf16[2048,256]{1,0:T(8,128)(2,1)} %wv_hbm.1, bf16[2048,128]{1,0:T(8,128)(2,1)} %wd_hbm.1, f32[8,64]{1,0:T(8,128)} %decay_in.1, ...), custom_call_target="tpu_custom_call" | custom-call | tf_op jit(solution)/shard_map/pallas_call | solution.py:621
  46.4 1.6 %copy.19 = bf16[32,2048]{1,0:T(8,128)(2,1)} copy(bf16[32,2048]{1,0:T(8,128)(2,1)} %shard_map.163) | data formatting | bytes 262144

commit v2 on v1

--- a/solution.py
+++ b/solution.py
@@ -338,6 +338,8 @@
 
     for i, tile in enumerate(turned(dot(x, wk[...]))):
         kv[0, 0, :, i * 128 : (i + 1) * 128] = tile.astype(BF16)
+    if gather and reach > 1:
+        w_relay(1)
     kv[0, 0, :, qw:] = dot(x, wv[...]).astype(BF16)
     drive = dot(x, wd[...]).astype(BF16).astype(F32)
 
@@ -350,9 +352,6 @@
         @pl.when(yi == 0)
         def _():
             k_across(0).start()
-
-    if gather and reach > 1:
-        w_relay(1)
 
     for which, ref in enumerate((ir, ii)):
         ref[...] = in_scale * dot(drive, block_map(in_map, which), HIGHEST)
@@ -454,10 +453,45 @@
             k_across(k).wait_recv()
             attend(k, 1)
 
+    def state_branch():
+        def enter(step, carry):
+            j = chain - step
+
+            def taken(carry):
+                cr, ci = carry
+                block = summary[j]
+                a, b = block[0:1], block[1:2]
+                return a * cr - b * ci + block[2:3], a * ci + b * cr + block[3:4]
+
+            @pl.when(j <= li)
+            def _():
+                summary_copy(j).wait_recv()
+
+            @pl.when(j > li)
+            def _():
+                summary[j] = jnp.zeros_like(summary[j])
+
+            return taken(carry)
+
+        cr, ci = lax.fori_loop(1, chain, enter, (zero, zero))
+        cr = jnp.where(head_of_chain, start_r, cr)
+        ci = jnp.where(head_of_chain, start_i, ci)
+        state_r = tr[...] * cr - ti[...] * ci + ir[...]
+        state_i = tr[...] * ci + ti[...] * cr + ii[...]
+        blocks = [block_map(out_map, w) for w in range(2)]
+        mixed = dot_t(state_r, blocks[0], HIGHEST) - dot_t(state_i, blocks[1], HIGHEST)
+        acts[:, :chans] = jax.nn.gelu(mixed + straight * drive).astype(BF16)
+
+    if reach == 1:
+        state_branch()
     for k in range(1, reach):
         relay_kv(k)
-        if gather and k >= 2:
+        if gather and k + 1 < reach - 1:
+            w_relay(k + 1)
+        if gather and k == reach - 1 and k > 1:
             w_relay(k)
+        if k == reach - 1:
+            state_branch()
         if fold == 2:
             attend_across(k - 1, (zi >= k - 1) if k > 1 else (yi == 1))
 
@@ -475,36 +509,12 @@
             diff * scale * sub_gain[...] * (1.0 - LAMBDA_INIT)
         ).astype(BF16)
 
-    def enter(step, carry):
-        j = chain - step
-
-        def taken(carry):
-            cr, ci = carry
-            block = summary[j]
-            a, b = block[0:1], block[1:2]
-            return a * cr - b * ci + block[2:3], a * ci + b * cr + block[3:4]
-
-        @pl.when(j <= li)
-        def _():
-            summary_copy(j).wait_recv()
-
-        @pl.when(j > li)
-        def _():
-            summary[j] = jnp.zeros_like(summary[j])
-
-        return taken(carry)
-
-    cr, ci = lax.fori_loop(1, chain, enter, (zero, zero))
-    cr = jnp.where(head_of_chain, start_r, cr)
-    ci = jnp.where(head_of_chain, start_i, ci)
-    state_r = tr[...] * cr - ti[...] * ci + ir[...]
-    state_i = tr[...] * ci + ti[...] * cr + ii[...]
-    blocks = [block_map(out_map, w) for w in range(2)]
-    mixed = dot_t(state_r, blocks[0], HIGHEST) - dot_t(state_i, blocks[1], HIGHEST)
-    acts[:, :chans] = jax.nn.gelu(mixed + straight * drive).astype(BF16)
-
     shares = [(r, c) for r in range(reach) for c in range(fold)] if gather else [(0, 0)]
-    order = sorted(range(len(shares)), key=lambda i: min(shares[i][0], reach - shares[i][0]))
+    shares.sort(key=lambda share: (share[0] > 0, share[1], share[0]))
+    order = range(len(shares))
+
+    def nearest_first(r):
+        return jnp.where(2 * zi >= reach, (reach - r) % reach, r) if r else 0
 
     def place(r, c):
         if not gather:
@@ -513,7 +523,7 @@
         return pl.multiple_of((lax.rem(zi + r, reach) * fold + y) * cols, 128)
 
     for i in order:
-        r, c = shares[i]
+        r, c = nearest_first(shares[i][0]), shares[i][1]
         if c:
             w_across(r).wait_recv()
         block = dot(acts[...], wo[r, c])
@@ -524,7 +534,7 @@
     summed = part[tp].astype(F32)
     for i in order:
         for d in range(1, tps):
-            r_copy(i, d, place(*shares[i])).wait_recv()
+            r_copy(i, d, place(nearest_first(shares[i][0]), shares[i][1])).wait_recv()
     for d in range(1, tps):
         summed = summed + landed[d].astype(F32)
     out[...] = summed.astype(BF16)
@@ -532,7 +542,7 @@
     for d in range(1, tps):
         x_copy(d).wait_send()
         for i in order:
-            r_copy(i, d, place(*shares[i])).wait_send()
+            r_copy(i, d, place(nearest_first(shares[i][0]), shares[i][1])).wait_send()
 
     def drain(d, _):
         @pl.when(li + d < chain)

time: 48.7 us -> 47.5 us (0.975)
  the two profiles are of different devices: /device:TPU:29 before, /device:TPU:27 now
where the time goes in v2:
time: 47.5 us; the launch traced here: 47.4 us
  Pallas kernels  45.8 us (96%)
  local copies, waits for them, and re-layouts  1.57 us (3%)
    pallas_call x1, Pallas kernels, local(): pl.pallas_call(functools.partial(kernel, (seqs, chain, tps, fold, gather)...  45.8 us
    unnamed x1, local copies, waits for them, and re-layouts  1.57 us

profile of v2, /device:TPU:27, one launch (start us, length us, event | category | flops | bytes accessed | tf_op | source)
XLA Modules:
  0.0 47.4 jit_solution(11043334341958671543)
XLA Ops:
  0.0 45.8 %shard_map.163 = bf16[32,2048]{1,0:T(8,128)(2,1)} custom-call(bf16[32,2048]{1,0:T(8,128)(2,1)} %tokens.1, f32[1,2048]{1,0:T(1,128)} %bitcast.10, bf16[2048,256]{1,0:T(8,128)(2,1)} %wq_hbm.1, bf16[2048,256]{1,0:T(8,128)(2,1)} %wk_hbm.1, bf16[2048,256]{1,0:T(8,128)(2,1)} %wv_hbm.1, bf16[2048,128]{1,0:T(8,128)(2,1)} %wd_hbm.1, f32[8,64]{1,0:T(8,128)} %decay_in.1, ...), custom_call_target="tpu_custom_call" | custom-call | tf_op jit(solution)/shard_map/pallas_call | solution.py:631
  45.8 1.6 %copy.19 = bf16[32,2048]{1,0:T(8,128)(2,1)} copy(bf16[32,2048]{1,0:T(8,128)(2,1)} %shard_map.163) | data formatting | bytes 262144
